TPU v7x, 32 devices: a whole 2x2x4 slice. The times are simulated.
32 devices in a mesh: dp: 2 (over x), kv: 8 (over z, y), tp: 2 (over core).
Axes of the slice: x: 2, y: 2, z: 4, core: 2. Of those that a mesh axis runs over, the one named last changes fastest.
Arguments:
- tokens: bfloat16 [48, 2048], P('dp', ('kv', 'tp')), may hold values from -21 to 21
- state: float32 [48, 8, 128, 128], P(('dp', 'kv'), 'tp'), may hold values from -3 to 3
- mix_gain: bfloat16 [2048], P(('kv', 'tp')), may hold values from 0.099609375 to 1.8984375
- w_query: bfloat16 [2048, 1024], P('kv', 'tp'), may hold values from -0.125 to 0.125
- w_key: bfloat16 [2048, 1024], P('kv', 'tp'), may hold values from -0.125 to 0.125
- w_value: bfloat16 [2048, 1024], P('kv', 'tp'), may hold values from -0.125 to 0.125
- w_beta: bfloat16 [2048, 8], P('kv', 'tp'), may hold values from -0.125 to 0.125
- w_decay: bfloat16 [2048, 8], P('kv', 'tp'), may hold values from -0.125 to 0.125
- decay_log: float32 [8], P('tp'), may hold values from -1.5 to 1
- head_gain: bfloat16 [128], replicated, may hold values from 0.099609375 to 1.8984375
- w_out: bfloat16 [1024, 2048], P('tp', 'kv'), may hold values from -0.1875 to 0.1875
- ff_gain: bfloat16 [2048], P(('kv', 'tp')), may hold values from 0.099609375 to 1.8984375
- w_up: bfloat16 [2048, 8192], P(None, ('kv', 'tp')), may hold values from -0.125 to 0.125
- w_down: bfloat16 [8192, 2048], P(('kv', 'tp')), may hold values from -0.09375 to 0.09375
Outputs:
- output: bfloat16 [48, 2048], P('dp', ('kv', 'tp'))
- new_state: float32 [48, 8, 128, 128], P(('dp', 'kv'), 'tp')
All inputs are finite; a program needn't handle non-finite values.
Results may differ from a plain program's by a relative error of at most 0.013.
Values may be sent and summed in bfloat16 or wider, within the bound.
A program may use at most 64 MiB of HBM per device.

v0:
```python
import jax
import jax.numpy as jnp
from jax import lax
from jax.sharding import PartitionSpec as P

D = 2048


def local(
    tokens,
    state,
    mix_gain,
    w_query,
    w_key,
    w_value,
    w_beta,
    w_decay,
    decay_log,
    head_gain,
    w_out,
    ff_gain,
    w_up,
    w_down,
):
    seq_count = state.shape[0]
    heads_local = state.shape[1]
    head_size = state.shape[2]
    tokens_wide, gain_wide = (
        lax.all_gather(tokens, "tp", axis=1, tiled=True),
        lax.all_gather(mix_gain[None, :], "tp", axis=1, tiled=True),
    )
    wide_float = tokens_wide.astype(jnp.float32)
    scaled = (wide_float * gain_wide.astype(jnp.float32)).astype(jnp.bfloat16)
    query_part = jnp.dot(scaled, w_query, preferred_element_type=jnp.float32)
    key_part = jnp.dot(scaled, w_key, preferred_element_type=jnp.float32)
    value_part = jnp.dot(scaled, w_value, preferred_element_type=jnp.float32)
    gate_part = jnp.concatenate(
        [
            jnp.dot(scaled, w_beta, preferred_element_type=jnp.float32),
            jnp.dot(scaled, w_decay, preferred_element_type=jnp.float32),
        ],
        axis=1,
    )
    square_part = jnp.sum(wide_float * wide_float, axis=1)
    query_sum, key_sum, value_sum, gate_sum, square_sum = (
        lax.psum_scatter(query_part, "kv", scatter_dimension=0, tiled=True),
        lax.psum_scatter(key_part, "kv", scatter_dimension=0, tiled=True),
        lax.psum_scatter(value_part, "kv", scatter_dimension=0, tiled=True),
        lax.psum_scatter(gate_part, "kv", scatter_dimension=0, tiled=True),
        lax.psum_scatter(square_part, "kv", scatter_dimension=0, tiled=True),
    )
    inverse = lax.rsqrt(square_sum / D + 1e-06)[:, None]
    query = (inverse * query_sum).reshape(seq_count, heads_local, head_size)
    key_rows = (inverse * key_sum).reshape(seq_count, heads_local, head_size)
    value = (inverse * value_sum).reshape(seq_count, heads_local, head_size)
    gates = inverse * gate_sum
    beta = jax.nn.sigmoid(gates[:, :heads_local])
    decay = -jnp.exp(decay_log)[None, :] * jax.nn.softplus(gates[:, heads_local:])
    qnorm = query * lax.rsqrt(jnp.sum(query * query, axis=-1, keepdims=True) + 1e-06)
    knorm = key_rows * lax.rsqrt(jnp.sum(key_rows * key_rows, axis=-1, keepdims=True) + 1e-06)
    kept = state * jnp.exp(decay)[:, :, None, None]
    predicted = jnp.sum(kept * knorm[:, :, :, None], axis=2)
    new_state = (
        kept + (beta[:, :, None] * knorm)[:, :, :, None] * (value - predicted)[:, :, None, :]
    )
    heads = jnp.sum(new_state * qnorm[:, :, :, None], axis=2) / jnp.sqrt(jnp.float32(head_size))
    normed = (
        heads
        * lax.rsqrt(jnp.mean(heads * heads, axis=-1, keepdims=True) + 1e-06)
        * head_gain.astype(jnp.float32)
    )
    normed = normed.astype(jnp.bfloat16).reshape(seq_count, heads_local * head_size)
    partial_mix = jnp.dot(
        lax.all_gather(normed, "kv", axis=0, tiled=True), w_out, preferred_element_type=jnp.float32
    )
    mixed = lax.psum_scatter(
        partial_mix.astype(jnp.bfloat16), "tp", scatter_dimension=1, tiled=True
    ).astype(jnp.float32)
    resid = (tokens.astype(jnp.float32) + mixed).astype(jnp.bfloat16)
    resid_float = resid.astype(jnp.float32)
    whole_rows = lax.all_gather(resid, ("kv", "tp"), axis=1, tiled=True)
    whole_gain = lax.all_gather(ff_gain[None, :], ("kv", "tp"), axis=1, tiled=True)
    whole_float = whole_rows.astype(jnp.float32)
    inverse2 = lax.rsqrt(jnp.mean(whole_float * whole_float, axis=1, keepdims=True) + 1e-06)
    scaled2 = (whole_float * whole_gain.astype(jnp.float32)).astype(jnp.bfloat16)
    up_rows = jnp.dot(scaled2, w_up, preferred_element_type=jnp.float32) * inverse2
    act = jnp.square(jax.nn.relu(up_rows)).astype(jnp.bfloat16)
    summed = lax.psum_scatter(
        lax.dot_general(w_down, act, (((0,), (1,)), ((), ())), preferred_element_type=jnp.float32),
        ("kv", "tp"),
        scatter_dimension=0,
        tiled=True,
    )
    results = (resid_float + summed.T).astype(jnp.bfloat16)
    return (results, new_state)


def solution(mesh):
    placed = (
        P("dp", ("kv", "tp")),
        P(("dp", "kv"), "tp", None, None),
        P(("kv", "tp")),
        P("kv", "tp"),
        P("kv", "tp"),
        P("kv", "tp"),
        P("kv", "tp"),
        P("kv", "tp"),
        P("tp"),
        P(),
        P("tp", "kv"),
        P(("kv", "tp")),
        P(None, ("kv", "tp")),
        P(("kv", "tp"), None),
    )
    return jax.shard_map(
        local,
        mesh=mesh,
        in_specs=placed,
        out_specs=(P("dp", ("kv", "tp")), P(("dp", "kv"), "tp", None, None)),
        check_vma=False,
    )
```

profile of v0, /device:TPU:0, one launch (start us, length us, event | category | flops | bytes accessed | tf_op | source)
XLA Modules:
  0.0 233.0 jit_solution(6209342007660774955)
XLA Ops:
  7.2 0.0 copy-start
  7.2 0.0 copy-start.1
  7.2 0.0 all-reduce.8.cloned.1.call-start
  7.2 2.2 all-gather.2
  9.5 2.0 all_gather.15
  11.5 0.6 fusion.9
  12.2 0.8 fusion.21
  13.0 0.8 fusion.23
  13.8 1.7 fusion.19
  15.5 1.7 fusion.17
  17.3 1.7 fusion.15
  19.0 0.6 pad_maximum_fusion
  19.6 0.0 all-reduce.8.cloned.1.call-update
  19.6 0.0 reduce-scatter.8.cloned.1.call-start
  19.7 0.7 convert_element_type.45
  20.3 1.2 dynamic-slice
  22.1 0.7 exponential_negate_fusion
  22.7 70.8 %all-reduce.8.cloned.1.call-done = (f32[24,512]{1,0:T(8,128)}, f32[24]{0:T(128)}, f32[24,512]{1,0:T(8,128)}, f32[24,8]{0,1:T(8,128)}, f32[24,512]{1,0:T(8,128)}) async-done(((f32[24,512]{1,0:T(8,128)}, f32[24]{0:T(128)}, f32[24,512]{1,0:T(8,128)}, f32[24,8]{0,1:T(8,128)}, f32[24,512]{1,0:T(8,128)}), (f32[24,512]{1,0:T(8,128)}, f32[24]{0:T(128)}, f32[24,512]{1,0:T(8,128)}, f32[24,8]{0,1:T(8,128)}, ...) | async-done | bytes 148336
  93.5 0.7 fusion.29
  94.3 0.8 dynamic-slice_multiply_fusion.3
  95.0 0.1 fusion.27
  95.1 0.1 copy.20
  95.2 0.9 dynamic-slice_multiply_fusion.2
  96.1 0.1 multiply_reduce_fusion.4
  96.2 0.1 copy.21
  96.3 0.1 multiply_reduce_fusion.3
  96.4 0.1 broadcast_multiply_fusion.2
  96.5 1.4 multiply_reduce_fusion.1
  98.0 0.0 copy-done.1
  98.0 1.4 multiply_reduce_fusion
  99.3 0.1 multiply_reduce_fusion.2
  99.4 0.1 multiply_bitcast_fusion
  99.5 30.6 %all-gather.3 = bf16[8,3,512]{2,1,0:T(4,128)(2,1)S(1)} all-gather(bf16[1,3,512]{2,1,0:T(4,128)(2,1)S(1)} %fusion.25), channel_id=1, replica_groups=mesh['dp'=2,'kv'=8,'tp'=2] {'kv'}, dimensions={0}, use_global_device_ids=true | all-gather | bytes 27648 | tf_op jit(solution)/shard_map/all_gather | solution.py:74
  130.2 0.2 convolution_convert_fusion
  130.3 0.7 copy.24
  131.0 0.0 reduce-scatter.8.cloned.1.call-update
  131.1 0.0 reduce-scatter.6.cloned.1.call-start
  131.1 0.0 copy-done.4
  131.1 20.4 %all-gather.4 = bf16[16,1,128]{2,1,0:T(2,128)(2,1)S(1)} all-gather(bf16[1,1,128]{2,1,0:T(2,128)(2,1)S(1)} %bitcast.44), channel_id=3, replica_groups=mesh['dp'=2,'kv'=8,'tp'=2] {'kv','tp'}, dimensions={0}, use_global_device_ids=true | all-gather | bytes 4352 | tf_op jit(solution)/shard_map/all_gather | solution.py:82
  151.5 0.0 reduce-scatter.8.cloned.1.call-done
  151.6 0.8 copy.25
  152.4 0.0 copy-done.3
  152.4 17.7 %all_gather.18 = bf16[24,2048]{1,0:T(8,128)(2,1)S(1)} all-gather(bf16[24,128]{1,0:T(8,128)(2,1)S(1)} %add_convert_fusion), channel_id=1, replica_groups=mesh['dp'=2,'kv'=8,'tp'=2] {'kv','tp'}, dimensions={1}, use_global_device_ids=true | all-gather | bytes 104448 | tf_op jit(solution)/shard_map/all_gather | solution.py:81
  170.1 0.1 fusion.4
  170.3 3.0 %convolution_bitcast_fusion = f32[2048,24]{0,1:T(8,128)} fusion(bf16[512,2048]{1,0:T(8,128)(2,1)S(1)} %copy-done, bf16[2048,512]{1,0:T(8,128)(2,1)} %param.26, bf16[24,2048]{1,0:T(8,128)(2,1)S(1)} %all_gather.18, f32[2048]{0:T(1024)S(1)} %bitcast.37, f32[24]{0:T(128)S(1)} %add_rsqrt_fusion.2), kind=kOutput, calls=%fused_computation | convolution fusion | flops 100859904 | bytes 4497504 | tf_op jit(solution)/shard_map/dot_general | solution.py:89
  173.3 0.0 reduce-scatter.6.cloned.1.call-update
  173.3 51.8 %reduce-scatter.6.cloned.1.call-done = f32[128,24]{0,1:T(8,128)} async-done(((f32[2048,24]{0,1:T(8,128)}), f32[128,24]{0,1:T(8,128)}) %reduce-scatter.6.cloned.1.call-update) | async-done | bytes 12304 | tf_op jit(solution)/shard_map/reduce_scatter | solution.py:88
  225.1 1.3 fusion.13
  (19 shorter events, 0.2 us)
Async XLA Ops:
  7.2 163.1 %copy-start = (bf16[512,2048]{1,0:T(8,128)(2,1)S(1)}, bf16[512,2048]{1,0:T(8,128)(2,1)}, u32[]{:S(2)}) copy-start(bf16[512,2048]{1,0:T(8,128)(2,1)} %param.27) | copy-start | bytes 6291460
  7.2 90.8 %copy-start.1 = (f32[3,4,128,128]{3,2,1,0:T(8,128)S(1)}, f32[3,4,128,128]{3,2,1,0:T(8,128)}, u32[]{:S(2)}) copy-start(f32[3,4,128,128]{3,2,1,0:T(8,128)} %param.15) | copy-start | bytes 2359300
  7.2 123.0 %copy-start.2 = (bf16[512,256]{1,0:T(8,128)(2,1)S(1)}, bf16[512,256]{1,0:T(8,128)(2,1)}, u32[]{:S(2)}) copy-start(bf16[512,256]{1,0:T(8,128)(2,1)} %param.24) | copy-start | bytes 786436
  7.2 86.3 %all-reduce.8.cloned.1.call-start = ((), (), s32[]{:S(2)}) async-start(), calls=%async_computation.4 | async-start | bytes 304128
  15.5 115.6 %copy-start.4 = (bf16[128]{0:T(256)(128)(2,1)S(1)}, bf16[128]{0:T(256)(128)(2,1)}, u32[]{:S(2)}) copy-start(bf16[128]{0:T(256)(128)(2,1)} %param.25) | copy-start | bytes 772
  15.5 136.9 %copy-start.3 = (bf16[24,128]{1,0:T(8,128)(2,1)S(1)}, bf16[24,128]{1,0:T(8,128)(2,1)}, u32[]{:S(2)}) copy-start(bf16[24,128]{1,0:T(8,128)(2,1)} %param.14) | copy-start | bytes 18436
  19.6 132.0 %reduce-scatter.8.cloned.1.call-start = ((), (), s32[]{:S(2)}) async-start(), calls=%async_computation.3 | async-start | bytes 98304
  131.1 94.1 %reduce-scatter.6.cloned.1.call-start = ((), (), s32[]{:S(2)}) async-start(), calls=%async_computation.2 | async-start | bytes 208896 | tf_op jit(solution)/shard_map/reduce_scatter | solution.py:88
Sparse Core Ops, SparseCore 0:
  19.7 73.7 all-reduce.7
  131.2 7.4 reduce-scatter.7
  173.4 51.6 reduce-scatter.5
where the time goes:
time: 234 us; the launch traced here: 233 us
  waiting for transfers between devices  123 us (53%)
  blocking collectives  73 us (31%)
  between operations  14.4 us (6%)
  matrix products  9.96 us (4%)
  other arithmetic  9.74 us (4%)
  local copies, waits for them, and re-layouts  3.05 us (1%)
    unnamed x5, waiting for transfers between devices  70.9 us
    reduce_scatter x1, waiting for transfers between devices, local(): lax.psum_scatter(lax.dot_general(w_down, act, (((0,), (1,)), ((), ())), p...  51.8 us
    all_gather x1, blocking collectives, local(): lax.all_gather(normed, 'kv', axis=0, tiled=True)  30.6 us
    all_gather x1, blocking collectives, local(): lax.all_gather(ff_gain[None, :], ('kv', 'tp'), axis=1, tiled=True)  20.4 us
    all_gather x1, blocking collectives, local(): whole_rows = lax.all_gather(resid, ('kv', 'tp'), axis=1, tiled=True)  17.7 us
  transfers between devices with their start and end apart: 3, of which 2 were waited for; matrix products, arithmetic and copies ran while one was open for 1% of the time, Pallas kernels for 0%

commit v1 on v0

--- a/solution.py
+++ b/solution.py
@@ -1,6 +1,10 @@
+import functools
+
 import jax
 import jax.numpy as jnp
 from jax import lax
+from jax.experimental import pallas as pl
+from jax.experimental.pallas import tpu as pltpu
 from jax.sharding import PartitionSpec as P
 
 D = 2048
@@ -95,6 +99,347 @@
     return (results, new_state)
 
 
+LANES = 128
+MESH = pl.DeviceIdType.MESH
+F32 = jnp.float32
+BF16 = jnp.bfloat16
+
+
+def fused_kernel(
+    n_kv,
+    n_tp,
+    tok_hbm, state_hbm, mg_hbm, wq_hbm, wk_hbm, wv_hbm, wb_hbm, wd_hbm, dl_hbm, hg_hbm,
+    wo_hbm, fg_hbm, wup_hbm, wdn_hbm,
+    out_ref, ns_hbm,
+    tok, state, mg, wqkv, wb, wd, dl, hg, wo, fg, wup, wdn,
+    x1_send, x1_recv, parts, rows, x2_send, x2_recv,
+    x3_send, x3_recv, heads_f32, left,
+    x5_send, x5_recv, x6_send, x6_recv,
+    load_sem, store_sem, x1_sems, wo_sems, s2, r2, s3, r3, s5, r5, s6, r6,
+):
+    kv = lax.axis_index("kv")
+    tp = lax.axis_index("tp")
+    other = 1 - tp
+    n_dev = n_kv * n_tp
+    me = kv * n_tp + tp
+    batch = tok.shape[0]
+    seqs, n_heads, size = state.shape[0], state.shape[1], state.shape[2]
+    wide = n_heads * size
+    d_model = n_dev * LANES
+    items = n_heads * seqs
+    stride2 = x2_send.shape[1]
+    stride3 = x3_recv.shape[1]
+
+    def place(device):
+        return {"kv": device // n_tp, "tp": lax.rem(device, n_tp)}
+
+    loads = [
+        (tok_hbm, tok), (mg_hbm, mg),
+        (wq_hbm, wqkv.at[:, 0:wide]),
+        (wk_hbm, wqkv.at[:, wide:2 * wide]),
+        (wv_hbm, wqkv.at[:, 2 * wide:3 * wide]),
+        (wb_hbm, wb), (wd_hbm, wd), (dl_hbm, dl), (hg_hbm, hg), (fg_hbm, fg),
+        (wo_hbm.at[:, pl.ds(pl.multiple_of(tp * LANES, LANES), LANES)], wo.at[tp]),
+        (state_hbm, state), (wup_hbm, wup), (wdn_hbm, wdn),
+    ]
+    copies = [
+        pltpu.make_async_copy(a, b, load_sem.at[i]) for i, (a, b) in enumerate(loads)
+    ]
+    for copy in copies:
+        copy.start()
+
+    barrier = pltpu.get_barrier_semaphore()
+    for step in range(1, n_dev):
+        pl.semaphore_signal(
+            barrier, inc=1, device_id=place(lax.rem(me + step, n_dev)), device_id_type=MESH
+        )
+    rows[...] = jnp.zeros_like(rows)
+    copies[0].wait()
+    copies[1].wait()
+    own = tok[...].astype(F32)
+    own_gain = mg[...].astype(F32)
+    x1_send[0:batch, :] = tok[...]
+    x1_send[batch:, :] = jnp.broadcast_to(own_gain, (x1_send.shape[0] - batch, LANES)).astype(BF16)
+    pl.semaphore_wait(barrier, n_dev - 1)
+
+    x1 = pltpu.make_async_remote_copy(
+        x1_send, x1_recv, x1_sems.at[0], x1_sems.at[1], device_id={"tp": other}, device_id_type=MESH
+    )
+    x1.start()
+    wo_copy = pltpu.make_async_remote_copy(
+        wo_hbm.at[:, pl.ds(pl.multiple_of(other * LANES, LANES), LANES)],
+        wo.at[tp], wo_sems.at[0], wo_sems.at[1], device_id={"tp": other}, device_id_type=MESH,
+    )
+    wo_copy.start()
+    for copy in copies[2:7]:
+        copy.wait()
+    gate_w = jnp.concatenate(
+        [
+            wb[...].astype(F32), wd[...].astype(F32),
+            jnp.zeros((wb.shape[0], LANES - 2 * n_heads), F32),
+        ],
+        axis=1,
+    ).astype(BF16)
+    own_scaled = own * own_gain
+    x1.wait()
+    far = x1_recv[0:batch, :].astype(F32)
+    far_scaled = far * x1_recv[batch:, :].astype(F32)[0:1, :]
+    first = tp == 0
+    scaled = jnp.concatenate(
+        [jnp.where(first, own_scaled, far_scaled), jnp.where(first, far_scaled, own_scaled)], axis=1
+    ).astype(BF16)
+    squares = jnp.sum(own * own + far * far, axis=1, keepdims=True)
+    gates = jnp.dot(scaled, gate_w, preferred_element_type=F32)
+    lane = lax.broadcasted_iota(jnp.int32, gates.shape, 1)
+    gates = jnp.where(lane == 2 * n_heads, squares, gates)
+    gates_hi = gates.astype(BF16).astype(F32)
+    chunks = 3 * n_heads
+    product = jnp.dot(scaled, wqkv[...], preferred_element_type=F32)
+    for c in range(chunks):
+        parts[c] = product[:, c * LANES:(c + 1) * LANES]
+    parts[chunks] = gates_hi
+    parts[chunks + 1] = gates - gates_hi
+    for c in range(chunks + 2):
+        for s in range(seqs):
+            rows[pl.ds(c * seqs + s, n_kv, stride=stride2), :] = parts[
+                c, pl.ds(s, n_kv, stride=seqs), :
+            ]
+    x2_send[...] = rows[...].reshape(x2_send.shape).astype(BF16)
+
+    sent2 = []
+    for step in range(1, n_kv):
+        peer = lax.rem(kv + step, n_kv)
+        copy = pltpu.make_async_remote_copy(
+            x2_send.at[peer], x2_recv.at[kv], s2.at[step], r2.at[kv],
+            device_id={"kv": peer}, device_id_type=MESH,
+        )
+        copy.start()
+        sent2.append(copy)
+    x2_recv[kv] = x2_send[kv]
+    for copy in copies[7:12]:
+        copy.wait()
+    for step in range(1, n_kv):
+        source = lax.rem(kv + step, n_kv)
+        pltpu.make_async_remote_copy(
+            x2_send.at[source], x2_recv.at[source], s2.at[step], r2.at[source],
+            device_id={"kv": source}, device_id_type=MESH,
+        ).wait_recv()
+    total = x2_recv[0].astype(F32)
+    for k in range(1, n_kv):
+        total = total + x2_recv[k].astype(F32)
+
+    g0 = 3 * items
+    gate = total[g0:g0 + seqs, :] + total[g0 + seqs:g0 + 2 * seqs, :]
+    inverse = lax.rsqrt(gate[:, 2 * n_heads:2 * n_heads + 1] / d_model + 1e-06)
+    gate = gate * inverse
+    beta = jax.nn.sigmoid(gate[:, 0:n_heads])
+    decay = jnp.exp(-jnp.exp(dl[...]) * jax.nn.softplus(gate[:, n_heads:2 * n_heads]))
+    inv_col = jnp.concatenate([inverse] * n_heads, axis=0)
+    query = total[0:items, :] * inv_col
+    key_rows = total[items:2 * items, :] * inv_col
+    value = total[2 * items:3 * items, :] * inv_col
+    qnorm = query * lax.rsqrt(jnp.sum(query * query, axis=1, keepdims=True) + 1e-06)
+    knorm = key_rows * lax.rsqrt(jnp.sum(key_rows * key_rows, axis=1, keepdims=True) + 1e-06)
+    fill = jnp.zeros((-items % 8, LANES), F32)
+    cols = jnp.transpose(jnp.concatenate([qnorm, fill, knorm, fill], axis=0))
+    k0 = items + fill.shape[0]
+    outs = []
+    for h in range(n_heads):
+        for s in range(seqs):
+            i = h * seqs + s
+            kept = state[s, h] * decay[s:s + 1, h:h + 1]
+            k_col = cols[:, k0 + i:k0 + i + 1]
+            q_col = cols[:, i:i + 1]
+            predicted = jnp.sum(kept * k_col, axis=0, keepdims=True)
+            delta = beta[s:s + 1, h:h + 1] * (value[i:i + 1, :] - predicted)
+            new = kept + k_col * delta
+            state[s, h] = new
+            outs.append(jnp.sum(new * q_col, axis=0, keepdims=True))
+    heads = jnp.concatenate(outs, axis=0) / jnp.sqrt(F32(size))
+    normed = (
+        heads * lax.rsqrt(jnp.mean(heads * heads, axis=1, keepdims=True) + 1e-06)
+        * hg[...].astype(F32)
+    )
+    x3_send[...] = jnp.concatenate(
+        [normed, jnp.broadcast_to(fg[...].astype(F32), (stride3 - items, LANES))], axis=0
+    ).astype(BF16)
+
+    sent3 = []
+    for step in range(1, n_dev):
+        copy = pltpu.make_async_remote_copy(
+            x3_send, x3_recv.at[me], s3.at[step], r3.at[me],
+            device_id=place(lax.rem(me + step, n_dev)), device_id_type=MESH,
+        )
+        copy.start()
+        sent3.append(copy)
+    ns_copy = pltpu.make_async_copy(state, ns_hbm, store_sem)
+    ns_copy.start()
+    x3_recv[me] = x3_send[...]
+    wo_copy.wait()
+    for step in range(1, n_dev):
+        source = lax.rem(me + step, n_dev)
+        pltpu.make_async_remote_copy(
+            x3_send, x3_recv.at[source], s3.at[step], r3.at[source],
+            device_id=place(source), device_id_type=MESH,
+        ).wait_recv()
+    heads_f32[...] = x3_recv[...].astype(F32).reshape(heads_f32.shape)
+    for t in range(n_tp):
+        for h in range(n_heads):
+            for s in range(seqs):
+                left[t * n_heads + h, pl.ds(s, n_kv, stride=seqs), :] = heads_f32[
+                    pl.ds(t * stride3 + h * seqs + s, n_kv, stride=n_tp * stride3), :
+                ]
+    mixed = None
+    for t in range(n_tp):
+        lhs = jnp.concatenate(
+            [left[t * n_heads + h].astype(BF16) for h in range(n_heads)], axis=1
+        )
+        half = jnp.dot(lhs, wo[t], preferred_element_type=F32).astype(BF16).astype(F32)
+        mixed = half if mixed is None else mixed + half
+    resid = (own + mixed).astype(BF16)
+    x5_send[...] = resid
+
+    sent5 = []
+    for step in range(1, n_dev):
+        copy = pltpu.make_async_remote_copy(
+            x5_send, x5_recv.at[me], s5.at[step], r5.at[me],
+            device_id=place(lax.rem(me + step, n_dev)), device_id_type=MESH,
+        )
+        copy.start()
+        sent5.append(copy)
+    x5_recv[me] = resid
+    copies[12].wait()
+
+    def arrived5(source):
+        pltpu.make_async_remote_copy(
+            x5_send, x5_recv.at[source], s5.at[0], r5.at[source],
+            device_id=place(source), device_id_type=MESH,
+        ).wait_recv()
+
+    up_rows = None
+    square2 = None
+    for step in range(n_kv):
+        chip = lax.rem(kv + step, n_kv)
+        if step == 0:
+            arrived5(kv * n_tp + other)
+        else:
+            for t in range(n_tp):
+                arrived5(chip * n_tp + t)
+        blocks = []
+        for t in range(n_tp):
+            block = x5_recv[chip * n_tp + t].astype(F32)
+            gain = x3_recv[chip * n_tp + t].astype(F32)[items:items + 1, :]
+            square2 = block * block if square2 is None else square2 + block * block
+            blocks.append((block * gain).astype(BF16))
+        deep = n_tp * LANES
+        term = jnp.dot(
+            jnp.concatenate(blocks, axis=1),
+            wup[pl.ds(pl.multiple_of(chip * deep, deep), deep), :],
+            preferred_element_type=F32,
+        )
+        up_rows = term if up_rows is None else up_rows + term
+    inverse2 = lax.rsqrt(jnp.sum(square2, axis=1, keepdims=True) / d_model + 1e-06)
+    act = jnp.square(jnp.maximum(up_rows * inverse2, 0.0)).astype(BF16)
+
+    copies[13].wait()
+    sent6 = []
+    own_sum = None
+    for step in range(1, n_kv + 1):
+        chip = lax.rem(kv + step, n_kv)
+        deep = n_tp * LANES
+        piece = jnp.dot(
+            act, wdn[:, pl.ds(pl.multiple_of(chip * deep, deep), deep)], preferred_element_type=F32
+        )
+        for t in range(n_tp):
+            x6_send[chip * n_tp + t] = piece[:, t * LANES:(t + 1) * LANES].astype(BF16)
+        if step < n_kv:
+            for t in range(n_tp):
+                copy = pltpu.make_async_remote_copy(
+                    x6_send.at[chip * n_tp + t], x6_recv.at[me],
+                    s6.at[step * n_tp + t], r6.at[me],
+                    device_id={"kv": chip, "tp": t}, device_id_type=MESH,
+                )
+                copy.start()
+                sent6.append(copy)
+        else:
+            copy = pltpu.make_async_remote_copy(
+                x6_send.at[chip * n_tp + other], x6_recv.at[me],
+                s6.at[0], r6.at[me], device_id={"tp": other}, device_id_type=MESH,
+            )
+            copy.start()
+            sent6.append(copy)
+            own_sum = jnp.where(first, piece[:, 0:LANES], piece[:, LANES:2 * LANES])
+    summed = resid.astype(F32) + own_sum
+    for step in range(1, n_dev):
+        source = lax.rem(me + step, n_dev)
+        pltpu.make_async_remote_copy(
+            x6_send.at[source], x6_recv.at[source], s6.at[0], r6.at[source],
+            device_id=place(source), device_id_type=MESH,
+        ).wait_recv()
+        summed = summed + x6_recv[source].astype(F32)
+    out_ref[...] = summed.astype(BF16)
+    for copy in sent2 + sent3 + sent5 + sent6:
+        copy.wait_send()
+    ns_copy.wait()
+
+
+def fused(n_kv, n_tp, *args):
+    (tokens, state, mix_gain, w_query, w_key, w_value, w_beta, w_decay, decay_log, head_gain,
+     w_out, ff_gain, w_up, w_down) = args
+    batch = tokens.shape[0]
+    seqs, n_heads = state.shape[:2]
+    items = seqs * n_heads
+    n_dev = n_kv * n_tp
+    chunks = 3 * n_heads + 2
+    stride2 = -(-chunks * seqs // 16) * 16
+    stride3 = -(-(items + 1) // 16) * 16
+    wide = w_query.shape[1]
+    operands = (
+        tokens, state, mix_gain[None, :], w_query, w_key, w_value, w_beta, w_decay,
+        decay_log[None, :], head_gain[None, :], w_out, ff_gain[None, :], w_up, w_down,
+    )
+    dma = pltpu.SemaphoreType.DMA
+    vmem = pltpu.VMEM
+    scratch = [
+        vmem(tokens.shape, BF16), vmem(state.shape, F32), vmem((1, LANES), BF16),
+        vmem((w_query.shape[0], 3 * wide), BF16), vmem(w_beta.shape, BF16),
+        vmem(w_decay.shape, BF16), vmem((1, n_heads), F32), vmem((1, LANES), BF16),
+        vmem((n_tp, w_out.shape[0], LANES), BF16), vmem((1, LANES), BF16),
+        vmem(w_up.shape, BF16), vmem(w_down.shape, BF16),
+        vmem((batch + 8, LANES), BF16), vmem((batch + 8, LANES), BF16),
+        vmem((chunks, batch, LANES), F32), vmem((n_kv * stride2, LANES), F32),
+        vmem((n_kv, stride2, LANES), BF16), vmem((n_kv, stride2, LANES), BF16),
+        vmem((stride3, LANES), BF16), vmem((n_dev, stride3, LANES), BF16),
+        vmem((n_dev * stride3, LANES), F32), vmem((n_tp * n_heads, batch, LANES), F32),
+        vmem((batch, LANES), BF16), vmem((n_dev, batch, LANES), BF16),
+        vmem((n_dev, batch, LANES), BF16), vmem((n_dev, batch, LANES), BF16),
+        dma((14,)), dma, dma((2,)), dma((2,)),
+        dma((n_kv,)), dma((n_kv,)), dma((n_dev,)), dma((n_dev,)),
+        dma((n_dev,)), dma((n_dev,)), dma((n_dev,)), dma((n_dev,)),
+    ]
+    return pl.pallas_call(
+        functools.partial(fused_kernel, n_kv, n_tp),
+        out_shape=(
+            jax.ShapeDtypeStruct(tokens.shape, BF16), jax.ShapeDtypeStruct(state.shape, F32),
+        ),
+        in_specs=[pl.BlockSpec(memory_space=pl.ANY)] * len(operands),
+        out_specs=(pl.BlockSpec(memory_space=pltpu.VMEM), pl.BlockSpec(memory_space=pl.ANY)),
+        scratch_shapes=scratch,
+        compiler_params=pltpu.CompilerParams(
+            collective_id=0, has_side_effects=True, vmem_limit_bytes=60 * 1024 * 1024
+        ),
+    )(*operands)
+
+
+def block_of(n_kv, n_tp, *args):
+    tokens, state = args[:2]
+    fits = (
+        tokens.shape[1] == LANES and n_kv == 8 and n_tp == 2
+        and state.shape[3] == LANES and tokens.shape[0] % 8 == 0
+    )
+    return fused(n_kv, n_tp, *args) if fits else local(*args)
+
+
 def solution(mesh):
     placed = (
         P("dp", ("kv", "tp")),
@@ -113,7 +458,7 @@
         P(("kv", "tp"), None),
     )
     return jax.shard_map(
-        local,
+        functools.partial(block_of, mesh.shape["kv"], mesh.shape["tp"]),
         mesh=mesh,
         in_specs=placed,
         out_specs=(P("dp", ("kv", "tp")), P(("dp", "kv"), "tp", None, None)),

time: 234 us -> 36 us (0.15)
  waiting for transfers between devices: 123 us -> 0 us
  blocking collectives: 73 us -> 0 us
  Pallas kernels: 0 us -> 28.9 us
  between operations: 14.4 us -> 0.64 us
  matrix products: 9.96 us -> 0 us
  other arithmetic: 9.74 us -> 0 us
  local copies, waits for them, and re-layouts: 3.05 us -> 6.21 us
    all_gather x5 -> x0, blocking collectives: 73 us -> none  [the longest x1 30.6 us: local(): lax.all_gather(normed, 'kv', axis=0, tiled=True)]
    unnamed x5 -> x0, waiting for transfers between devices: 70.9 us -> none
    reduce_scatter x1 -> x0, waiting for transfers between devices: 51.8 us -> none  [local(): lax.psum_scatter(lax.dot_general(w_down, act, (((0,), (1,)), ((), ())), p...]
    pallas_call x0 -> x1, Pallas kernels: none -> 28.9 us  [fused(): pl.pallas_call(functools.partial(fused_kernel, n_kv, n_tp), out_shape=(ja...]
    dot_general x7 -> x0, matrix products: 9.96 us -> none  [the longest x1 3.02 us: local(): lax.dot_general(w_down, act, (((0,), (1,)), ((), ())), preferred_element_...]
    reduce_sum x7 -> x0, other arithmetic: 3.84 us -> none  [the longest x1 1.44 us: local(): predicted = jnp.sum(kept * knorm[:, :, :, None], axis=2)]
    unnamed x14 -> x4, local copies, waits for them, and re-layouts: 2.81 us -> 6.21 us
  transfers between devices with their start and end apart: 3 -> 0, of which waited for: 2 -> 0; matrix products, arithmetic and copies ran while one was open for 1% -> 0% of each run, Pallas kernels for 0% -> 0%
where the time goes in v1:
time: 36 us; the launch traced here: 35.7 us
  Pallas kernels  28.9 us (80%)
  local copies, waits for them, and re-layouts  6.21 us (17%)
  between operations  0.64 us (2%)
    pallas_call x1, Pallas kernels, fused(): pl.pallas_call(functools.partial(fused_kernel, n_kv, n_tp), out_shape=(ja...  28.9 us
    unnamed x4, local copies, waits for them, and re-layouts  6.21 us

profile of v1, /device:TPU:0, one launch (start us, length us, event | category | flops | bytes accessed | tf_op | source)
XLA Modules:
  0.0 35.7 jit_solution(64797586661921677)
XLA Ops:
  0.6 1.4 %copy.16.wb_hbm = bf16[256,4]{1,0:T(8,128)(2,1)} copy(bf16[256,4]{0,1:T(4,128)(2,1)} %param.20) | data formatting | bytes 4096 | tf_op args[6]
  2.1 1.4 %copy.17.wd_hbm = bf16[256,4]{1,0:T(8,128)(2,1)} copy(bf16[256,4]{0,1:T(4,128)(2,1)} %param.21) | data formatting | bytes 4096 | tf_op args[7]
  3.5 28.9 %shard_map.149 = (bf16[24,128]{1,0:T(8,128)(2,1)}, f32[3,4,128,128]{3,2,1,0:T(8,128)}) custom-call(bf16[24,128]{1,0:T(8,128)(2,1)} %tok_hbm.1, f32[3,4,128,128]{3,2,1,0:T(8,128)} %state_hbm.1, bf16[1,128]{1,0:T(2,128)(2,1)} %bitcast.4, bf16[256,512]{1,0:T(8,128)(2,1)} %wq_hbm.1, bf16[256,512]{1,0:T(8,128)(2,1)} %wk_hbm.1, bf16[256,512]{1,0:T(8,128)(2,1)} %wv_hbm.1, ...), custom_call_target="tpu_custom_call" | custom-call | tf_op jit(solution)/shard_map/pallas_call | solution.py:420
  32.4 1.3 %copy.20 = bf16[24,128]{1,0:T(8,128)(2,1)} copy(bf16[24,128]{1,0:T(8,128)(2,1)} %get-tuple-element.4) | data formatting | bytes 12288
  33.7 2.1 %copy.21 = f32[3,4,128,128]{3,2,1,0:T(8,128)} copy(f32[3,4,128,128]{3,2,1,0:T(8,128)} %get-tuple-element.5) | data formatting | bytes 1572864

commit v2 on v1

--- a/solution.py
+++ b/solution.py
@@ -110,12 +110,12 @@
     n_tp,
     tok_hbm, state_hbm, mg_hbm, wq_hbm, wk_hbm, wv_hbm, wb_hbm, wd_hbm, dl_hbm, hg_hbm,
     wo_hbm, fg_hbm, wup_hbm, wdn_hbm,
-    out_ref, ns_hbm,
-    tok, state, mg, wqkv, wb, wd, dl, hg, wo, fg, wup, wdn,
+    out_ref, state,
+    tok, mg, wqkv, wb, wd, dl, hg, wo, fg, wup, wdn,
     x1_send, x1_recv, parts, rows, x2_send, x2_recv,
     x3_send, x3_recv, heads_f32, left,
     x5_send, x5_recv, x6_send, x6_recv,
-    load_sem, store_sem, x1_sems, wo_sems, s2, r2, s3, r3, s5, r5, s6, r6,
+    load_sem, x1_sems, wo_sems, s2, r2, s3, r3, s5, r5, s6, r6,
 ):
     kv = lax.axis_index("kv")
     tp = lax.axis_index("tp")
@@ -129,6 +129,10 @@
     items = n_heads * seqs
     stride2 = x2_send.shape[1]
     stride3 = x3_recv.shape[1]
+
+    far_first = sorted(range(1, n_kv), key=lambda step: -min(step, n_kv - step))
+    far_devices = [step * n_tp + t for step in far_first for t in range(n_tp)]
+    partner = kv * n_tp + other
 
     def place(device):
         return {"kv": device // n_tp, "tp": lax.rem(device, n_tp)}
@@ -176,9 +180,9 @@
     gate_w = jnp.concatenate(
         [
             wb[...].astype(F32), wd[...].astype(F32),
-            jnp.zeros((wb.shape[0], LANES - 2 * n_heads), F32),
+            jnp.zeros((LANES - 2 * n_heads, wb.shape[1]), F32),
         ],
-        axis=1,
+        axis=0,
     ).astype(BF16)
     own_scaled = own * own_gain
     x1.wait()
@@ -189,7 +193,9 @@
         [jnp.where(first, own_scaled, far_scaled), jnp.where(first, far_scaled, own_scaled)], axis=1
     ).astype(BF16)
     squares = jnp.sum(own * own + far * far, axis=1, keepdims=True)
-    gates = jnp.dot(scaled, gate_w, preferred_element_type=F32)
+    gates = lax.dot_general(
+        scaled, gate_w, (((1,), (1,)), ((), ())), preferred_element_type=F32
+    )
     lane = lax.broadcasted_iota(jnp.int32, gates.shape, 1)
     gates = jnp.where(lane == 2 * n_heads, squares, gates)
     gates_hi = gates.astype(BF16).astype(F32)
@@ -207,7 +213,7 @@
     x2_send[...] = rows[...].reshape(x2_send.shape).astype(BF16)
 
     sent2 = []
-    for step in range(1, n_kv):
+    for step in far_first:
         peer = lax.rem(kv + step, n_kv)
         copy = pltpu.make_async_remote_copy(
             x2_send.at[peer], x2_recv.at[kv], s2.at[step], r2.at[kv],
@@ -243,19 +249,20 @@
     fill = jnp.zeros((-items % 8, LANES), F32)
     cols = jnp.transpose(jnp.concatenate([qnorm, fill, knorm, fill], axis=0))
     k0 = items + fill.shape[0]
-    outs = []
+    along_k, along_q = [], []
     for h in range(n_heads):
         for s in range(seqs):
             i = h * seqs + s
-            kept = state[s, h] * decay[s:s + 1, h:h + 1]
-            k_col = cols[:, k0 + i:k0 + i + 1]
-            q_col = cols[:, i:i + 1]
-            predicted = jnp.sum(kept * k_col, axis=0, keepdims=True)
-            delta = beta[s:s + 1, h:h + 1] * (value[i:i + 1, :] - predicted)
-            new = kept + k_col * delta
-            state[s, h] = new
-            outs.append(jnp.sum(new * q_col, axis=0, keepdims=True))
-    heads = jnp.concatenate(outs, axis=0) / jnp.sqrt(F32(size))
+            before = state[s, h]
+            along_k.append(jnp.sum(before * cols[:, k0 + i:k0 + i + 1], axis=0, keepdims=True))
+            along_q.append(jnp.sum(before * cols[:, i:i + 1], axis=0, keepdims=True))
+    beta_col = jnp.concatenate([beta[:, h:h + 1] for h in range(n_heads)], axis=0)
+    decay_col = jnp.concatenate([decay[:, h:h + 1] for h in range(n_heads)], axis=0)
+    delta = beta_col * (value - decay_col * jnp.concatenate(along_k, axis=0))
+    heads = (
+        decay_col * jnp.concatenate(along_q, axis=0)
+        + jnp.sum(qnorm * knorm, axis=1, keepdims=True) * delta
+    ) / jnp.sqrt(F32(size))
     normed = (
         heads * lax.rsqrt(jnp.mean(heads * heads, axis=1, keepdims=True) + 1e-06)
         * hg[...].astype(F32)
@@ -265,15 +272,21 @@
     ).astype(BF16)
 
     sent3 = []
-    for step in range(1, n_dev):
+    for step in far_devices + [0]:
+        peer = lax.rem(kv * n_tp + step, n_dev) if step else partner
         copy = pltpu.make_async_remote_copy(
             x3_send, x3_recv.at[me], s3.at[step], r3.at[me],
-            device_id=place(lax.rem(me + step, n_dev)), device_id_type=MESH,
+            device_id=place(peer), device_id_type=MESH,
         )
         copy.start()
         sent3.append(copy)
-    ns_copy = pltpu.make_async_copy(state, ns_hbm, store_sem)
-    ns_copy.start()
+    for h in range(n_heads):
+        for s in range(seqs):
+            i = h * seqs + s
+            state[s, h] = (
+                state[s, h] * decay[s:s + 1, h:h + 1]
+                + cols[:, k0 + i:k0 + i + 1] * delta[i:i + 1, :]
+            )
     x3_recv[me] = x3_send[...]
     wo_copy.wait()
     for step in range(1, n_dev):
@@ -300,10 +313,11 @@
     x5_send[...] = resid
 
     sent5 = []
-    for step in range(1, n_dev):
+    for step in far_devices + [0]:
+        peer = lax.rem(kv * n_tp + step, n_dev) if step else partner
         copy = pltpu.make_async_remote_copy(
             x5_send, x5_recv.at[me], s5.at[step], r5.at[me],
-            device_id=place(lax.rem(me + step, n_dev)), device_id_type=MESH,
+            device_id=place(peer), device_id_type=MESH,
         )
         copy.start()
         sent5.append(copy)
@@ -318,7 +332,7 @@
 
     up_rows = None
     square2 = None
-    for step in range(n_kv):
+    for step in [0] + far_first[::-1]:
         chip = lax.rem(kv + step, n_kv)
         if step == 0:
             arrived5(kv * n_tp + other)
@@ -344,7 +358,7 @@
     copies[13].wait()
     sent6 = []
     own_sum = None
-    for step in range(1, n_kv + 1):
+    for step in far_first + [n_kv]:
         chip = lax.rem(kv + step, n_kv)
         deep = n_tp * LANES
         piece = jnp.dot(
@@ -380,7 +394,6 @@
     out_ref[...] = summed.astype(BF16)
     for copy in sent2 + sent3 + sent5 + sent6:
         copy.wait_send()
-    ns_copy.wait()
 
 
 def fused(n_kv, n_tp, *args):
@@ -395,15 +408,16 @@
     stride3 = -(-(items + 1) // 16) * 16
     wide = w_query.shape[1]
     operands = (
-        tokens, state, mix_gain[None, :], w_query, w_key, w_value, w_beta, w_decay,
+        tokens, state, mix_gain[None, :], w_query, w_key, w_value, w_beta.T, w_decay.T,
         decay_log[None, :], head_gain[None, :], w_out, ff_gain[None, :], w_up, w_down,
     )
+    operands = [pltpu.with_memory_space_constraint(x, pltpu.HBM) for x in operands]
     dma = pltpu.SemaphoreType.DMA
     vmem = pltpu.VMEM
     scratch = [
-        vmem(tokens.shape, BF16), vmem(state.shape, F32), vmem((1, LANES), BF16),
-        vmem((w_query.shape[0], 3 * wide), BF16), vmem(w_beta.shape, BF16),
-        vmem(w_decay.shape, BF16), vmem((1, n_heads), F32), vmem((1, LANES), BF16),
+        vmem(tokens.shape, BF16), vmem((1, LANES), BF16),
+        vmem((w_query.shape[0], 3 * wide), BF16), vmem(w_beta.shape[::-1], BF16),
+        vmem(w_decay.shape[::-1], BF16), vmem((1, n_heads), F32), vmem((1, LANES), BF16),
         vmem((n_tp, w_out.shape[0], LANES), BF16), vmem((1, LANES), BF16),
         vmem(w_up.shape, BF16), vmem(w_down.shape, BF16),
         vmem((batch + 8, LANES), BF16), vmem((batch + 8, LANES), BF16),
@@ -413,20 +427,20 @@
         vmem((n_dev * stride3, LANES), F32), vmem((n_tp * n_heads, batch, LANES), F32),
         vmem((batch, LANES), BF16), vmem((n_dev, batch, LANES), BF16),
         vmem((n_dev, batch, LANES), BF16), vmem((n_dev, batch, LANES), BF16),
-        dma((14,)), dma, dma((2,)), dma((2,)),
+        dma((14,)), dma((2,)), dma((2,)),
         dma((n_kv,)), dma((n_kv,)), dma((n_dev,)), dma((n_dev,)),
         dma((n_dev,)), dma((n_dev,)), dma((n_dev,)), dma((n_dev,)),
     ]
     return pl.pallas_call(
         functools.partial(fused_kernel, n_kv, n_tp),
         out_shape=(
-            jax.ShapeDtypeStruct(tokens.shape, BF16), jax.ShapeDtypeStruct(state.shape, F32),
+            pltpu.VMEM(tokens.shape, BF16), pltpu.VMEM(state.shape, F32),
         ),
-        in_specs=[pl.BlockSpec(memory_space=pl.ANY)] * len(operands),
-        out_specs=(pl.BlockSpec(memory_space=pltpu.VMEM), pl.BlockSpec(memory_space=pl.ANY)),
+        in_specs=[pl.BlockSpec(memory_space=pltpu.HBM)] * len(operands),
+        out_specs=(pl.BlockSpec(memory_space=pltpu.VMEM), pl.BlockSpec(memory_space=pltpu.VMEM)),
         scratch_shapes=scratch,
         compiler_params=pltpu.CompilerParams(
-            collective_id=0, has_side_effects=True, vmem_limit_bytes=60 * 1024 * 1024
+            collective_id=0, has_side_effects=True, vmem_limit_bytes=67043328 - 786432 - 16384
         ),
     )(*operands)
 

time: 36 us -> 32 us (0.89)
  local copies, waits for them, and re-layouts: 6.21 us -> 1.47 us
  Pallas kernels: 28.9 us -> 29.7 us
    unnamed x4 -> x2, local copies, waits for them, and re-layouts: 6.21 us -> 1.47 us
    pallas_call x1, Pallas kernels: 28.9 us -> 29.7 us  [fused(): pl.pallas_call(functools.partial(fused_kernel, n_kv, n_tp), out_shape=(pl...]
where the time goes in v2:
time: 32 us; the launch traced here: 31.8 us
  Pallas kernels  29.7 us (93%)
  local copies, waits for them, and re-layouts  1.47 us (5%)
  between operations  0.64 us (2%)
    pallas_call x1, Pallas kernels, fused(): pl.pallas_call(functools.partial(fused_kernel, n_kv, n_tp), out_shape=(pl...  29.7 us
    unnamed x2, local copies, waits for them, and re-layouts  1.47 us

profile of v2, /device:TPU:0, one launch (start us, length us, event | category | flops | bytes accessed | tf_op | source)
XLA Modules:
  0.0 31.8 jit_solution(9263736320052330875)
XLA Ops:
  0.6 29.7 %shard_map.149 = (bf16[24,128]{1,0:T(8,128)(2,1)S(1)}, f32[3,4,128,128]{3,2,1,0:T(8,128)S(1)}) custom-call(bf16[24,128]{1,0:T(8,128)(2,1)} %tok_hbm.1, f32[3,4,128,128]{3,2,1,0:T(8,128)} %state_hbm.1, bf16[1,128]{1,0:T(2,128)(2,1)} %bitcast.8, bf16[256,512]{1,0:T(8,128)(2,1)} %wq_hbm.1, bf16[256,512]{1,0:T(8,128)(2,1)} %wk_hbm.1, bf16[256,512]{1,0:T(8,128)(2,1)} %wv_hbm.1, ...), custom_call_target="tpu_custom_call" | custom-call | tf_op jit(solution)/shard_map/pallas_call | solution.py:434
  30.3 0.6 %copy.18 = bf16[24,128]{1,0:T(8,128)(2,1)} copy(bf16[24,128]{1,0:T(8,128)(2,1)S(1)} %get-tuple-element.2) | data formatting | bytes 12288
  30.9 0.9 %copy.19 = f32[3,4,128,128]{3,2,1,0:T(8,128)} copy(f32[3,4,128,128]{3,2,1,0:T(8,128)S(1)} %get-tuple-element.3) | data formatting | bytes 1572864

commit v3 on v2

--- a/solution.py
+++ b/solution.py
@@ -115,7 +115,7 @@
     x1_send, x1_recv, parts, rows, x2_send, x2_recv,
     x3_send, x3_recv, heads_f32, left,
     x5_send, x5_recv, x6_send, x6_recv,
-    load_sem, x1_sems, wo_sems, s2, r2, s3, r3, s5, r5, s6, r6,
+    load_sem, go_sem, x1_sems, wo_sems, s2, r2, s3, r3, s5, r5, s6, r6,
 ):
     kv = lax.axis_index("kv")
     tp = lax.axis_index("tp")
@@ -153,9 +153,17 @@
         copy.start()
 
     barrier = pltpu.get_barrier_semaphore()
-    for step in range(1, n_dev):
+    lead = n_tp - 1
+    leads = tp == lead
+
+    @pl.when(leads)
+    def _():
+        pl.semaphore_signal(barrier, inc=1, device_id={"tp": other}, device_id_type=MESH)
+
+    for step in far_first:
         pl.semaphore_signal(
-            barrier, inc=1, device_id=place(lax.rem(me + step, n_dev)), device_id_type=MESH
+            barrier, inc=1, device_id={"kv": lax.rem(kv + step, n_kv), "tp": lead},
+            device_id_type=MESH,
         )
     rows[...] = jnp.zeros_like(rows)
     copies[0].wait()
@@ -164,11 +172,19 @@
     own_gain = mg[...].astype(F32)
     x1_send[0:batch, :] = tok[...]
     x1_send[batch:, :] = jnp.broadcast_to(own_gain, (x1_send.shape[0] - batch, LANES)).astype(BF16)
-    pl.semaphore_wait(barrier, n_dev - 1)
 
     x1 = pltpu.make_async_remote_copy(
         x1_send, x1_recv, x1_sems.at[0], x1_sems.at[1], device_id={"tp": other}, device_id_type=MESH
     )
+
+    @pl.when(jnp.logical_not(leads))
+    def _():
+        pl.semaphore_wait(barrier, 1)
+
+    @pl.when(leads)
+    def _():
+        x1.wait_recv()
+
     x1.start()
     wo_copy = pltpu.make_async_remote_copy(
         wo_hbm.at[:, pl.ds(pl.multiple_of(other * LANES, LANES), LANES)],
@@ -177,15 +193,21 @@
     wo_copy.start()
     for copy in copies[2:7]:
         copy.wait()
+    low = LANES // 2
     gate_w = jnp.concatenate(
         [
+            wb[...].astype(F32), wd[...].astype(F32), jnp.zeros((low - 2 * n_heads, wb.shape[1]), F32),
             wb[...].astype(F32), wd[...].astype(F32),
-            jnp.zeros((LANES - 2 * n_heads, wb.shape[1]), F32),
+            jnp.zeros((LANES - low - 2 * n_heads, wb.shape[1]), F32),
         ],
         axis=0,
     ).astype(BF16)
     own_scaled = own * own_gain
-    x1.wait()
+
+    @pl.when(jnp.logical_not(leads))
+    def _():
+        x1.wait_recv()
+
     far = x1_recv[0:batch, :].astype(F32)
     far_scaled = far * x1_recv[batch:, :].astype(F32)[0:1, :]
     first = tp == 0
@@ -197,20 +219,28 @@
         scaled, gate_w, (((1,), (1,)), ((), ())), preferred_element_type=F32
     )
     lane = lax.broadcasted_iota(jnp.int32, gates.shape, 1)
-    gates = jnp.where(lane == 2 * n_heads, squares, gates)
+    gates = jnp.where(lax.rem(lane, low) == 2 * n_heads, squares, gates)
     gates_hi = gates.astype(BF16).astype(F32)
     chunks = 3 * n_heads
     product = jnp.dot(scaled, wqkv[...], preferred_element_type=F32)
     for c in range(chunks):
         parts[c] = product[:, c * LANES:(c + 1) * LANES]
-    parts[chunks] = gates_hi
-    parts[chunks + 1] = gates - gates_hi
-    for c in range(chunks + 2):
+    parts[chunks] = jnp.where(lane < low, gates_hi, gates - gates_hi)
+    for c in range(chunks + 1):
         for s in range(seqs):
             rows[pl.ds(c * seqs + s, n_kv, stride=stride2), :] = parts[
                 c, pl.ds(s, n_kv, stride=seqs), :
             ]
     x2_send[...] = rows[...].reshape(x2_send.shape).astype(BF16)
+
+    @pl.when(leads)
+    def _():
+        pl.semaphore_wait(barrier, n_dev - n_tp)
+        pl.semaphore_signal(go_sem, inc=1, device_id={"tp": other}, device_id_type=MESH)
+
+    @pl.when(jnp.logical_not(leads))
+    def _():
+        pl.semaphore_wait(go_sem, 1)
 
     sent2 = []
     for step in far_first:
@@ -235,7 +265,8 @@
         total = total + x2_recv[k].astype(F32)
 
     g0 = 3 * items
-    gate = total[g0:g0 + seqs, :] + total[g0 + seqs:g0 + 2 * seqs, :]
+    gate = total[g0:g0 + seqs, :]
+    gate = gate[:, 0:low] + gate[:, low:]
     inverse = lax.rsqrt(gate[:, 2 * n_heads:2 * n_heads + 1] / d_model + 1e-06)
     gate = gate * inverse
     beta = jax.nn.sigmoid(gate[:, 0:n_heads])
@@ -392,8 +423,37 @@
         ).wait_recv()
         summed = summed + x6_recv[source].astype(F32)
     out_ref[...] = summed.astype(BF16)
-    for copy in sent2 + sent3 + sent5 + sent6:
+    for copy in [x1] + sent2 + sent3 + sent5 + sent6:
         copy.wait_send()
+
+
+def store_kernel(out_ref, state_ref, out_hbm, state_hbm, sems):
+    pieces = [(out_ref, out_hbm)] + [
+        (state_ref.at[s, h], state_hbm.at[s, h])
+        for s in range(state_ref.shape[0])
+        for h in range(state_ref.shape[1])
+    ]
+    copies = [
+        pltpu.make_async_copy(a, b, sems.at[i]) for i, (a, b) in enumerate(pieces)
+    ]
+    for copy in copies:
+        copy.start()
+    for copy in copies:
+        copy.wait()
+
+
+def store_results(output, state):
+    return pl.pallas_call(
+        store_kernel,
+        out_shape=(
+            jax.ShapeDtypeStruct(output.shape, output.dtype),
+            jax.ShapeDtypeStruct(state.shape, state.dtype),
+        ),
+        in_specs=[pl.BlockSpec(memory_space=pltpu.VMEM)] * 2,
+        out_specs=(pl.BlockSpec(memory_space=pl.ANY),) * 2,
+        scratch_shapes=[pltpu.SemaphoreType.DMA((1 + state.shape[0] * state.shape[1],))],
+        compiler_params=pltpu.CompilerParams(vmem_limit_bytes=1024 * 1024),
+    )(output, state)
 
 
 def fused(n_kv, n_tp, *args):
@@ -403,8 +463,8 @@
     seqs, n_heads = state.shape[:2]
     items = seqs * n_heads
     n_dev = n_kv * n_tp
-    chunks = 3 * n_heads + 2
-    stride2 = -(-chunks * seqs // 16) * 16
+    chunks = 3 * n_heads + 1
+    stride2 = -(-chunks * seqs // 8) * 8
     stride3 = -(-(items + 1) // 16) * 16
     wide = w_query.shape[1]
     operands = (
@@ -427,11 +487,11 @@
         vmem((n_dev * stride3, LANES), F32), vmem((n_tp * n_heads, batch, LANES), F32),
         vmem((batch, LANES), BF16), vmem((n_dev, batch, LANES), BF16),
         vmem((n_dev, batch, LANES), BF16), vmem((n_dev, batch, LANES), BF16),
-        dma((14,)), dma((2,)), dma((2,)),
+        dma((14,)), pltpu.SemaphoreType.REGULAR, dma((2,)), dma((2,)),
         dma((n_kv,)), dma((n_kv,)), dma((n_dev,)), dma((n_dev,)),
         dma((n_dev,)), dma((n_dev,)), dma((n_dev,)), dma((n_dev,)),
     ]
-    return pl.pallas_call(
+    results = pl.pallas_call(
         functools.partial(fused_kernel, n_kv, n_tp),
         out_shape=(
             pltpu.VMEM(tokens.shape, BF16), pltpu.VMEM(state.shape, F32),
@@ -443,6 +503,7 @@
             collective_id=0, has_side_effects=True, vmem_limit_bytes=67043328 - 786432 - 16384
         ),
     )(*operands)
+    return store_results(*results)
 
 
 def block_of(n_kv, n_tp, *args):

time: 32 us -> 30.1 us (0.941)
  local copies, waits for them, and re-layouts: 1.47 us -> 0 us
  Pallas kernels: 29.7 us -> 29.3 us
    unnamed x2 -> x0, local copies, waits for them, and re-layouts: 1.47 us -> none
    pallas_call x1, Pallas kernels: 29.7 us -> 28.3 us  [fused(): pl.pallas_call(functools.partial(fused_kernel, n_kv, n_tp), out_shape=(pl...]
    pallas_call x0 -> x1, Pallas kernels: none -> 0.98 us  [store_results(): pl.pallas_call(store_kernel, out_shape=(jax.ShapeDtypeStruct(output.shape...]
where the time goes in v3:
time: 30.1 us; the launch traced here: 29.9 us
  Pallas kernels  29.3 us (97%)
  between operations  0.64 us (2%)
    pallas_call x1, Pallas kernels, fused(): pl.pallas_call(functools.partial(fused_kernel, n_kv, n_tp), out_shape=(pl...  28.3 us
    pallas_call x1, Pallas kernels, store_results(): pl.pallas_call(store_kernel, out_shape=(jax.ShapeDtypeStruct(output.shape...  0.98 us

profile of v3, /device:TPU:0, one launch (start us, length us, event | category | flops | bytes accessed | tf_op | source)
XLA Modules:
  0.0 29.9 jit_solution(4857022181951449807)
XLA Ops:
  0.6 28.3 %shard_map.149 = (bf16[24,128]{1,0:T(8,128)(2,1)S(1)}, f32[3,4,128,128]{3,2,1,0:T(8,128)S(1)}) custom-call(bf16[24,128]{1,0:T(8,128)(2,1)} %tok_hbm.1, f32[3,4,128,128]{3,2,1,0:T(8,128)} %state_hbm.1, bf16[1,128]{1,0:T(2,128)(2,1)} %bitcast.8, bf16[256,512]{1,0:T(8,128)(2,1)} %wq_hbm.1, bf16[256,512]{1,0:T(8,128)(2,1)} %wk_hbm.1, bf16[256,512]{1,0:T(8,128)(2,1)} %wv_hbm.1, ...), custom_call_target="tpu_custom_call" | custom-call | tf_op jit(solution)/shard_map/pallas_call | solution.py:494
  28.9 1.0 %shard_map.150 = (bf16[24,128]{1,0:T(8,128)(2,1)}, f32[3,4,128,128]{3,2,1,0:T(8,128)}) custom-call(bf16[24,128]{1,0:T(8,128)(2,1)S(1)} %get-tuple-element.4.out_ref, f32[3,4,128,128]{3,2,1,0:T(8,128)S(1)} %get-tuple-element.5.state_ref), custom_call_target="tpu_custom_call" | custom-call | tf_op jit(solution)/shard_map/pallas_call | solution.py:446
